TPU v7x, 32 devices: a whole 2x2x4 slice. The times are simulated.
32 devices in a mesh: grp: 2 (over y), sp: 4 (over z), tp: 4 (over x, core).
Axes of the slice: x: 2, y: 2, z: 4, core: 2. Of those that a mesh axis runs over, the one named last changes fastest.
Arguments:
- residual: bfloat16 [4096, 2048], P(('grp', 'sp')), parts along dimension 0, may hold values from -6 to 6
- values: bfloat16 [4096, 4096], P(('grp', 'sp'), 'tp'), parts along dimension 0, may hold values from -6 to 6
- out_gate: bfloat16 [4096, 4096], P(('grp', 'sp'), 'tp'), parts along dimension 0, may hold values from -6 to 6
- writes: bfloat16 [4096, 1024], P(('grp', 'sp'), 'tp'), parts along dimension 0, may hold values from -6 to 6
- reads: bfloat16 [4096, 1024], P(('grp', 'sp'), 'tp'), parts along dimension 0, may hold values from -6 to 6
- step_raw: bfloat16 [64, 4096], P('tp', ('grp', 'sp')), parts along dimension 1, may hold values from -4.5 to 4.5
- decay_rate: float32 [64], P('tp'), may hold values from 0 to 0.1
- decay_jump: float32 [64, 4096], P('tp', ('grp', 'sp')), parts along dimension 1, may hold values from -0.7 to 0
- documents: int32 [4096], P(('grp', 'sp')), parts along dimension 0, may hold values from 0 to 1, never falling along the last dimension, each value on 1 to 1536 neighbouring positions
- taps_values: bfloat16 [4, 4096], P(None, 'tp'), may hold values from -3 to 3
- taps_write: bfloat16 [4, 1024], P(None, 'tp'), may hold values from -3 to 3
- taps_read: bfloat16 [4, 1024], P(None, 'tp'), may hold values from -3 to 3
- mixer_gain: bfloat16 [4096], P('tp'), may hold values from 0.099609375 to 1.8984375
- mixer_out: bfloat16 [4096, 2048], P('tp'), may hold values from -0.09375 to 0.09375
- channel_gain: bfloat16 [2048], replicated, may hold values from 0.099609375 to 1.8984375
- gate_weight: bfloat16 [2048, 5632], P('sp', 'tp'), may hold values from -0.125 to 0.125
- up_weight: bfloat16 [2048, 5632], P('sp', 'tp'), may hold values from -0.125 to 0.125
- down_rows: bfloat16 [2048, 5632], P('sp', 'tp'), may hold values from -0.078125 to 0.078125
Outputs:
- layer_out: bfloat16 [4096, 2048], P(('grp', 'sp'), 'tp'), parts along dimension 0
There are 2 independent parts, one for each index of `grp`. A program takes and returns all parts, laid end to end along the dimension named above; an argument that names none is the same for every part. Nothing has to cross between parts.
Inputs may be any that keep to these rules, and one draw needn't show every extreme that they name: `documents`: document numbers never fall along the sequence; a document starts where the number changes, and is one to 1536 positions long.
All inputs are finite; a program needn't handle non-finite values.
Results may differ from a plain program's by a relative error of at most 0.017.
Values may be sent and summed in bfloat16 or wider, within the bound.
A program may use at most 64 MiB of HBM per device.

v0:
```python
import jax
import jax.numpy as jnp
from jax import lax
from jax.sharding import PartitionSpec as P

HEADS = 64
GROUPS = 8
BLOCK = 128


norm_eps = 1e-06


def from_behind(value, axis, by):
    peers = lax.axis_size(axis)
    pairs = [(i, i + by) for i in range(peers) if 0 <= i + by < peers]
    return lax.ppermute(value, axis, pairs)


def prefix(value, axis, combine, identity):
    peers, index = (lax.axis_size(axis), lax.axis_index(axis))
    everything = jax.tree.map(
        lambda part, kind: lax.all_gather(part.astype(kind), axis),
        value,
        (jnp.bfloat16, jnp.bfloat16, jnp.bfloat16, jnp.bfloat16),
    )
    start = jax.tree.map(
        lambda part, zero: jnp.broadcast_to(jnp.asarray(zero, part.dtype), part.shape),
        value,
        identity,
    )

    def step(k, before):
        reached = k < index
        new = combine(
            before, jax.tree.map(lambda part, own: part[k].astype(own.dtype), everything, value)
        )
        return jax.tree.map(lambda a, b: jnp.where(reached, a, b), new, before)

    return lax.fori_loop(0, peers, step, start)


def short_filter(rows, row_docs, taps):
    width = taps.shape[0]
    count = rows.shape[0] - width + 1
    own_docs = row_docs[width - 1 :]
    total = jnp.zeros((count, rows.shape[1]), jnp.float32)
    for offset in range(width):
        alive = (row_docs[offset : offset + count] == own_docs).astype(jnp.float32)
        total = (
            total
            + rows[offset : offset + count].astype(jnp.float32)
            * taps[offset].astype(jnp.float32)[None, :]
            * alive[:, None]
        )
    return jax.nn.silu(total).astype(jnp.bfloat16)


def block_pieces(values, writes, reads, step_size, log_decay, segment, heads_per, block):
    span = values.shape[0]
    block_count = span // block
    heads = step_size.shape[0]
    groups = heads // heads_per
    head_size = values.shape[1] // heads
    state_size = writes.shape[1] // groups
    value_blocks = values.reshape(block_count, block, groups, heads_per, head_size)
    write_blocks = writes.reshape(block_count, block, groups, state_size)
    read_blocks = reads.reshape(block_count, block, groups, state_size)
    block_docs = segment.reshape(block_count, block)
    step_blocks = step_size.reshape(groups, heads_per, block_count, block)
    running = jnp.cumsum(log_decay.reshape(groups, heads_per, block_count, block), axis=3)
    target = lax.broadcasted_iota(jnp.int32, (block, block), 0)
    source = lax.broadcasted_iota(jnp.int32, (block, block), 1)
    allowed = (target >= source)[None] & (block_docs[:, :, None] == block_docs[:, None, :])
    scores = jnp.einsum(
        "kign,kjgn->gkij", read_blocks, write_blocks, preferred_element_type=jnp.float32
    )
    spread = running[..., :, None] - running[..., None, :]
    decay = jnp.exp(jnp.where(allowed[None, None], spread, -jnp.inf))
    weights = (decay * scores[:, None] * step_blocks[..., None, :]).astype(jnp.bfloat16)
    inner = jnp.einsum(
        "gekij,kjgep->kigep", weights, value_blocks, preferred_element_type=jnp.float32
    )
    last_total = running[..., -1]
    same_end = (block_docs == block_docs[:, -1:]).astype(jnp.float32)
    end_factor = jnp.exp(last_total[..., None] - running) * step_blocks * same_end[None, None]
    scaled = (
        value_blocks.astype(jnp.float32) * jnp.transpose(end_factor, (2, 3, 0, 1))[..., None]
    ).astype(jnp.bfloat16)
    states = jnp.einsum(
        "kjgep,kjgn->kgepn", scaled, write_blocks, preferred_element_type=jnp.float32
    )
    return (inner, states, last_total, running, block_docs)


def block_passing(last_total, block_docs, prior_docs):
    return jnp.exp(last_total) * (block_docs[:, -1] == prior_docs).astype(jnp.float32)[None, None]


def carry_states(states, passing, start):

    def advance(held, entry):
        factor, fresh = entry
        return (factor[..., None, None] * held + fresh, held)

    final, entering = lax.scan(advance, start, (jnp.moveaxis(passing, 2, 0), states))
    return (entering, final)


def read_states(reads, entering, running, block_docs, prior_docs):
    block_count, block = block_docs.shape
    groups = entering.shape[1]
    read_blocks = reads.astype(jnp.float32).reshape(block_count, block, groups, -1)
    alive = (block_docs == prior_docs[:, None]).astype(jnp.float32)
    reach = jnp.exp(running) * alive[None, None]
    taken = jnp.einsum("kign,kgepn->kigep", read_blocks, entering, precision=lax.Precision.HIGHEST)
    return taken * jnp.transpose(reach, (2, 3, 0, 1))[..., None]


def join_states(earlier, later):
    early_decay, early_state, early_first, early_last = earlier
    late_decay, late_state, late_first, late_last = later
    link = ((late_first == early_last) | (early_last < 0.0) | (late_first < 0.0)).astype(
        jnp.float32
    )
    carried = late_decay * link
    return (
        early_decay * carried,
        late_state + carried[..., None, None] * early_state,
        jnp.where(early_first < 0.0, late_first, early_first),
        jnp.where(late_last < 0.0, early_last, late_last),
    )


def down_product(hidden, rows):
    return lax.dot_general(
        hidden, rows, (((1,), (1,)), ((), ())), preferred_element_type=jnp.float32
    )


def on_device(
    residual,
    values,
    out_gate,
    writes,
    reads,
    step_raw,
    decay_rate,
    decay_jump,
    documents,
    taps_values,
    taps_write,
    taps_read,
    mixer_gain,
    mixer_out,
    channel_gain,
    gate_weight,
    up_weight,
    down_rows,
):
    tokens = values.shape[0]
    edge = taps_values.shape[0] - 1
    segment = documents.astype(jnp.float32)
    before = from_behind(
        (
            values[tokens - edge :],
            writes[tokens - edge :],
            reads[tokens - edge :],
            segment[tokens - edge :].astype(jnp.bfloat16),
        ),
        "sp",
        1,
    )
    row_docs = jnp.concatenate([before[3].astype(jnp.float32), segment])
    short_values = short_filter(jnp.concatenate([before[0], values]), row_docs, taps_values)
    short_writes = short_filter(jnp.concatenate([before[1], writes]), row_docs, taps_write)
    short_reads = short_filter(jnp.concatenate([before[2], reads]), row_docs, taps_read)
    step_size = jax.nn.softplus(step_raw.astype(jnp.float32))
    log_decay = decay_jump - decay_rate[:, None] * step_size
    heads_per = HEADS // GROUPS
    inner, states, last_total, running, block_docs = block_pieces(
        short_values, short_writes, short_reads, step_size, log_decay, segment, heads_per, BLOCK
    )
    groups = states.shape[1]
    local_prior = jnp.concatenate([jnp.full((1,), -1.0, jnp.float32), block_docs[:-1, -1]])
    zero_state = jnp.zeros(states.shape[1:], jnp.float32)
    entering, final = carry_states(
        states, block_passing(last_total, block_docs, local_prior), zero_state
    )
    whole_decay = jnp.exp(jnp.sum(last_total, axis=2)) * (segment[0] == segment[-1]).astype(
        jnp.float32
    )
    identity = (
        jnp.ones_like(whole_decay),
        zero_state,
        jnp.full((1,), -1.0, jnp.float32),
        jnp.full((1,), -1.0, jnp.float32),
    )
    scanned = prefix((whole_decay, final, segment[:1], segment[-1:]), "sp", join_states, identity)
    held = scanned[1]
    prior_docs = jnp.concatenate([scanned[3], block_docs[:-1, -1]])
    passing_in = block_passing(last_total, block_docs, prior_docs)
    gains = jnp.cumprod(passing_in, axis=2)
    gains = jnp.concatenate([jnp.ones_like(gains[..., :1]), gains[..., :-1]], axis=2)
    entering = entering + jnp.moveaxis(gains, 2, 0)[..., None, None] * held[None]
    mixed = inner + read_states(short_reads, entering, running, block_docs, prior_docs)
    gated = mixed.reshape(tokens, -1) * jax.nn.silu(out_gate.astype(jnp.float32))
    grouped = gated.reshape(tokens, groups, -1)
    grouped = grouped * lax.rsqrt(jnp.mean(grouped * grouped, axis=2, keepdims=True) + norm_eps)
    mixer_in = (grouped.reshape(tokens, -1) * mixer_gain.astype(jnp.float32)[None, :]).astype(
        jnp.bfloat16
    )
    partial_value = jnp.dot(mixer_in, mixer_out, preferred_element_type=jnp.float32)
    share = residual.shape[1] // lax.axis_size("tp")
    mix = lax.psum(partial_value.astype(jnp.bfloat16), "tp").astype(jnp.float32)
    after = (residual.astype(jnp.float32) + mix).astype(jnp.bfloat16)
    own_after = lax.dynamic_slice_in_dim(after, lax.axis_index("tp") * share, share, 1)
    after_wide = after.astype(jnp.float32)
    normal = after_wide * lax.rsqrt(
        jnp.mean(after_wide * after_wide, axis=1, keepdims=True) + norm_eps
    )
    normal = (normal * channel_gain.astype(jnp.float32)[None, :]).astype(jnp.bfloat16)
    late_weights = (
        lax.all_gather(gate_weight, "sp", axis=0, tiled=True),
        lax.all_gather(up_weight, "sp", axis=0, tiled=True),
        lax.all_gather(down_rows, "sp", axis=0, tiled=True),
    )
    gate = jnp.dot(normal, late_weights[0], preferred_element_type=jnp.float32)
    up = jnp.dot(normal, late_weights[1], preferred_element_type=jnp.float32)
    hidden = (jax.nn.silu(gate) * up).astype(jnp.bfloat16)
    down = down_product(hidden, late_weights[2])
    down_share = lax.psum_scatter(
        down.astype(jnp.bfloat16), "tp", scatter_dimension=1, tiled=True
    ).astype(jnp.float32)
    return (own_after.astype(jnp.float32) + down_share).astype(jnp.bfloat16)


def solution(mesh):
    return jax.shard_map(
        on_device,
        mesh=mesh,
        in_specs=(
            P(("grp", "sp"), None),
            P(("grp", "sp"), "tp"),
            P(("grp", "sp"), "tp"),
            P(("grp", "sp"), "tp"),
            P(("grp", "sp"), "tp"),
            P("tp", ("grp", "sp")),
            P("tp"),
            P("tp", ("grp", "sp")),
            P(("grp", "sp")),
            P(None, "tp"),
            P(None, "tp"),
            P(None, "tp"),
            P("tp"),
            P("tp", None),
            P(),
            P("sp", "tp"),
            P("sp", "tp"),
            P("sp", "tp"),
        ),
        out_specs=P(("grp", "sp"), "tp"),
        check_vma=False,
    )
```

profile of v0, /device:TPU:0, one launch (start us, length us, event | category | flops | bytes accessed | tf_op | source)
XLA Modules:
  0.0 526.1 jit_solution(8923508315370118888)
XLA Ops:
  6.6 0.7 convert_bitcast_fusion
  7.4 4.9 collective-permute-start.1
  12.4 0.7 slice.114
  13.3 3.5 collective-permute-start
  16.8 0.7 slice.134
  17.5 3.5 collective-permute-start.3
  21.0 1.3 slice.126
  22.3 2.5 collective-permute-start.2
  24.7 1.5 copy.69
  27.9 2.3 reduce_window_sum.11
  30.2 0.7 slice_reduce_fusion
  32.6 2.6 multiply_convert_fusion.3
  37.0 3.9 while.29
  37.0 0.8 bitcast_dynamic-update-slice_fusion.2
  38.0 0.8 bitcast_dynamic-update-slice_fusion.2
  38.9 0.8 bitcast_dynamic-update-slice_fusion.2
  39.9 0.8 bitcast_dynamic-update-slice_fusion.2
  40.9 0.7 convert_element_type.285
  41.8 0.6 fusion.55
  44.4 1.3 dynamic-update-slice
  45.7 1.4 dynamic-update-slice.1
  47.9 9.0 %all-reduce.3 = (bf16[4]{0:T(256)(128)(2,1)S(1)}, bf16[4]{0:T(256)(128)(2,1)S(1)}) all-reduce(bf16[4]{0:T(256)(128)(2,1)S(1)} %dynamic-update-slice, bf16[4]{0:T(256)(128)(2,1)S(1)} %dynamic-update-slice.1), channel_id=4, replica_groups=mesh['grp'=2,'sp'=4,'tp'=4] {'sp'}, use_global_device_ids=true, to_apply=%add.1 | all-reduce | flops 8 | bytes 32
  56.9 9.9 %all-gather.4 = bf16[4,2,8]{2,1,0:T(2,128)(2,1)S(1)} all-gather(bf16[1,2,8]{2,1,0:T(2,128)(2,1)S(1)} %fusion.52), channel_id=3, replica_groups=mesh['grp'=2,'sp'=4,'tp'=4] {'sp'}, dimensions={0}, use_global_device_ids=true | all-gather | bytes 160 | tf_op jit(solution)/shard_map/all_gather | solution.py:23
  66.8 1.6 copy.85
  68.5 1.2 multiply_convert_fusion.5
  70.1 3.8 fusion.5
  73.9 17.4 %while.30 = (s32[]{:T(128)}, f32[2,8,64,128]{3,2,1,0:T(8,128)S(1)}, f32[1]{0:T(128)}, s32[]{:T(128)}, bf16[4,2,8,64,128]{4,3,2,1,0:T(8,128)(2,1)}, /*index=5*/bf...) while((s32[]{:T(128)}, f32[2,8,64,128]{3,2,1,0:T(8,128)S(1)}, ...), condition=%wide.region_5.6_spmd.clone, body=%wide.region_4.5_spmd.clone.sunk | while | flops 655405 | bytes 1311098 | solution.py:40
  73.9 0.6 constant_dynamic-slice_fusion.7
  75.8 1.1 fusion.66
  80.2 1.1 fusion.66
  84.5 1.1 fusion.66
  88.9 1.1 fusion.66
  91.6 3.6 fusion.12
  95.2 1.4 copy.84
  96.6 0.7 bitcast_reduce_fusion
  97.3 0.7 fusion.11
  98.0 1.5 copy-done.27
  99.5 3.8 convolution_convert_fusion
  103.4 0.7 all-gather.10.cloned.1.call-update
  105.5 47.6 %all-reduce.6.cloned.1.call-done = bf16[512,2048]{1,0:T(8,128)(2,1)} async-done(((bf16[512,2048]{1,0:T(8,128)(2,1)}), bf16[512,2048]{1,0:T(8,128)(2,1)}) %all-reduce.6.cloned.1.call-update) | async-done | bytes 2097168 | tf_op jit(solution)/shard_map/psum | solution.py:215
  153.1 3.2 fusion.1
  156.4 105.2 %all-gather.10.cloned.1.call-done = bf16[2048,1408]{1,0:T(8,128)(2,1)} async-done(((bf16[512,1408]{1,0:T(8,128)(2,1)}), bf16[2048,1408]{1,0:T(8,128)(2,1)}) %all-gather.10.cloned.1.call-update) | async-done | bytes 5767184 | tf_op jit(solution)/shard_map/all_gather | solution.py:224
  261.5 7.6 %fusion.33 = f32[512,1408]{1,0:T(8,128)} fusion(bf16[2048,1408]{1,0:T(8,128)(2,1)} %all-gather.10.cloned.1.call-done, bf16[512,2048]{1,0:T(8,128)(2,1)S(1)} %get-tuple-element.273, f32[2048]{0:T(1024)S(1)} %convert_element_type.302, f32[512]{0:T(512)S(1)} %add_rsqrt_fusion.1), kind=kOutput, calls=%fused_computation.57 | convolution fusion | flops 2956984320 | bytes 10758144 | tf_op jit(solution)/shard_map/dot_general | solution.py:228
  269.2 98.8 %all-gather.12.cloned.1.call-done = bf16[2048,1408]{1,0:T(8,128)(2,1)} async-done(((bf16[512,1408]{1,0:T(8,128)(2,1)}), bf16[2048,1408]{1,0:T(8,128)(2,1)}) %all-gather.12.cloned.1.call-update) | async-done | bytes 5767184 | tf_op jit(solution)/shard_map/all_gather | solution.py:225
  367.9 106.4 %all-gather.14.cloned.1.call-done = bf16[2048,1408]{1,0:T(8,128)(2,1)} async-done(((bf16[512,1408]{1,0:T(8,128)(2,1)}), bf16[2048,1408]{1,0:T(8,128)(2,1)}) %all-gather.14.cloned.1.call-update) | async-done | bytes 5767184 | tf_op jit(solution)/shard_map/all_gather | solution.py:226
  474.3 13.3 %convolution_convert_fusion.1 = bf16[512,2048]{1,0:T(8,128)(2,1)} fusion(bf16[2048,1408]{1,0:T(8,128)(2,1)} %all-gather.14.cloned.1.call-done, bf16[2048,1408]{1,0:T(8,128)(2,1)} %all-gather.12.cloned.1.call-done, f32[512,1408]{1,0:T(8,128)} %fusion.33, bf16[512,2048]{1,0:T(8,128)(2,1)S(1)} %get-tuple-element.273, f32[2048]{0:T(1024)S(1)} %convert_element_type.302, ...), kind=kOutput, calls=%fused_computation.19 | convolution fusion | flops 5915148288 | bytes 18622464 | tf_op jit(solution)/shard_map/dot_general | solution.py:136
  487.7 29.6 %reduce-scatter.2.cloned.1.call-done = bf16[512,512]{1,0:T(8,128)(2,1)} async-done(((bf16[512,2048]{1,0:T(8,128)(2,1)}), bf16[512,512]{1,0:T(8,128)(2,1)}) %reduce-scatter.2.cloned.1.call-update) | async-done | bytes 524304 | tf_op jit(solution)/shard_map/reduce_scatter | solution.py:232
  517.3 2.0 add_convert_fusion.1
  (131 shorter events, 11.4 us)
Async XLA Ops:
  6.5 24.4 %copy-start.12 = (s32[512]{0:T(512)S(1)}, s32[512]{0:T(512)}, u32[]{:S(2)}) copy-start(s32[512]{0:T(512)} %param.30) | copy-start | bytes 6148
  6.5 25.6 %copy-start.2 = (bf16[512,256]{1,0:T(8,128)(2,1)S(1)}, bf16[512,256]{1,0:T(8,128)(2,1)}, u32[]{:S(2)}) copy-start(bf16[512,256]{1,0:T(8,128)(2,1)} %param.25) | copy-start | bytes 786436
  6.5 20.7 %copy-start.11 = (bf16[4,1024]{1,0:T(4,128)(2,1)S(1)}, bf16[4,1024]{1,0:T(4,128)(2,1)}, u32[]{:S(2)}) copy-start(bf16[4,1024]{1,0:T(4,128)(2,1)} %param.31) | copy-start | bytes 24580
  6.5 20.7 %copy-start.4 = (bf16[16,512]{1,0:T(8,128)(2,1)S(1)}, bf16[16,512]{1,0:T(8,128)(2,1)}, u32[]{:S(2)}) copy-start(bf16[16,512]{1,0:T(8,128)(2,1)} %param.27) | copy-start | bytes 49156
  6.5 20.7 %copy-start.26 = (f32[16]{0:T(128)S(1)}, f32[16]{0:T(128)}, u32[]{:S(2)}) copy-start(f32[16]{0:T(128)} %param.28) | copy-start | bytes 196
  6.5 20.7 %copy-start.10 = (f32[16,512]{1,0:T(8,128)S(1)}, f32[16,512]{1,0:T(8,128)}, u32[]{:S(2)}) copy-start(f32[16,512]{1,0:T(8,128)} %param.29) | copy-start | bytes 98308
  6.6 24.6 %copy-start.16 = (bf16[4,256]{1,0:T(4,128)(2,1)S(1)}, bf16[4,256]{1,0:T(4,128)(2,1)}, u32[]{:S(2)}) copy-start(bf16[4,256]{1,0:T(4,128)(2,1)} %param.32) | copy-start | bytes 6148
  6.6 67.3 %all-gather.16.cloned.1.call-start = ((), (), s32[]{:S(2)}) async-start(), calls=%async_computation.6 | async-start | bytes 1310720 | tf_op jit(solution)/shard_map/all_gather | solution.py:23
  7.4 24.5 %collective-permute-start.1 = (bf16[3]{0:T(256)(128)(2,1)S(1)}, bf16[3]{0:T(256)(128)(2,1)S(1)}, u32[]{:S(2)}, u32[]{:S(2)}) collective-permute-start(bf16[3]{0:T(256)(128)(2,1)S(1)} %slice.117), channel_id=1, source_target_pairs={{0,4},{4,8},{8,12},{1,5},{5,9},{9,13},{2,6},{6,10},{10,14},{3,7},{... | collective-permute-start | bytes 26 | tf_op jit(solution)/shard_map/ppermute | solution.py:17
  13.3 19.3 %collective-permute-start = (bf16[3,1024]{0,1:T(8,128)(2,1)S(1)}, bf16[3,1024]{0,1:T(8,128)(2,1)S(1)}, u32[]{:S(2)}, u32[]{:S(2)}) collective-permute-start(bf16[3,1024]{0,1:T(8,128)(2,1)S(1)} %copy.68), channel_id=1, source_target_pairs={{0,4},{4,8},{8,12},{1,5},{5,9},{9,13},{2,6},{6,10},{10,14},{3,7},{... | collective-permute-start | bytes 18440 | tf_op jit(solution)/shard_map/ppermute | solution.py:17
  17.5 14.6 %collective-permute-start.3 = (bf16[3,256]{1,0:T(4,128)(2,1)S(1)}, bf16[3,256]{1,0:T(4,128)(2,1)S(1)}, u32[]{:S(2)}, u32[]{:S(2)}) collective-permute-start(bf16[3,256]{1,0:T(4,128)(2,1)S(1)} %slice.134), channel_id=1, source_target_pairs={{0,4},{4,8},{8,12},{1,5},{5,9},{9,13},{2,6},{6,10},{10,14},{3,7},{... | collective-permute-start | bytes 4616 | tf_op jit(solution)/shard_map/ppermute | solution.py:17
  22.3 46.1 %collective-permute-start.2 = (bf16[3,256]{1,0:T(4,128)(2,1)}, bf16[3,256]{1,0:T(4,128)(2,1)}, u32[]{:S(2)}, u32[]{:S(2)}) collective-permute-start(bf16[3,256]{1,0:T(4,128)(2,1)} %slice.126), channel_id=1, source_target_pairs={{0,4},{4,8},{8,12},{1,5},{5,9},{9,13},{2,6},{6,10},{10,14},{3,7},{... | collective-permute-start | bytes 4616 | tf_op jit(solution)/shard_map/ppermute | solution.py:17
  26.4 5.5 %copy-start.14 = (f32[4]{0:T(128)}, f32[4]{0:T(128)S(1)}, u32[]{:S(2)}) copy-start(f32[4]{0:T(128)S(1)} %slice_reduce_fusion.3) | copy-start | bytes 52
  26.6 4.5 copy-start.18
  32.1 3.4 copy-start.6
  32.1 3.4 copy-start.8
  35.5 1.0 copy-start
  36.9 6.8 %copy-start.28 = (u32[32]{0:T(128)S(1)}, u32[32]{0:T(128)}, u32[]{:S(2)}) copy-start(u32[32]{0:T(128)} %constant.93) | copy-start | bytes 388
  36.9 10.2 %copy-start.17 = (bf16[4,256]{1,0:T(4,128)(2,1)S(1)}, bf16[4,256]{1,0:T(4,128)(2,1)}, u32[]{:S(2)}) copy-start(bf16[4,256]{1,0:T(4,128)(2,1)} %param.33) | copy-start | bytes 6148
  36.9 10.7 %copy-start.5 = (pred[128,128]{1,0:T(8,128)(4,1)S(1)}, pred[128,128]{1,0:T(8,128)(4,1)}, u32[]{:S(2)}) copy-start(pred[128,128]{1,0:T(8,128)(4,1)} %iota_compare_fusion) | copy-start | bytes 49156
  36.9 10.9 %copy-start.24 = (f32[2,8]{1,0:T(2,128)S(1)}, f32[2,8]{1,0:T(2,128)}, u32[]{:S(2)}) copy-start(f32[2,8]{1,0:T(2,128)} %get-tuple-element.242) | copy-start | bytes 196
  40.9 27.5 %copy-start.25 = (bf16[1024]{0:T(1024)(128)(2,1)S(1)}, bf16[1024]{0:T(1024)(128)(2,1)}, u32[]{:S(2)}) copy-start(bf16[1024]{0:T(1024)(128)(2,1)} %param.34) | copy-start | bytes 6148
  40.9 27.5 %copy-start.3 = (bf16[512,256]{1,0:T(8,128)(2,1)S(1)}, bf16[512,256]{1,0:T(8,128)(2,1)}, u32[]{:S(2)}) copy-start(bf16[512,256]{1,0:T(8,128)(2,1)} %param.26) | copy-start | bytes 786436
  40.9 27.5 %copy-start.7 = (f32[512]{0:T(512)S(1)}, f32[512]{0:T(512)}, u32[]{:S(2)}) copy-start(f32[512]{0:T(512)} %copy-done.6) | copy-start | bytes 6148
  40.9 27.5 %copy-start.9 = (f32[512]{0:T(512)S(1)}, f32[512]{0:T(512)}, u32[]{:S(2)}) copy-start(f32[512]{0:T(512)} %copy-done.8) | copy-start | bytes 6148
  41.7 111.4 %all-reduce.6.cloned.1.call-start = ((), (), s32[]{:S(2)}) async-start(), calls=%async_computation.1 | async-start | bytes 4194304 | tf_op jit(solution)/shard_map/psum | solution.py:215
  47.8 20.6 %copy-start.20 = (f32[1,256]{1,0:T(1,128)S(1)}, f32[1,256]{1,0:T(1,128)}, u32[]{:S(2)}) copy-start(f32[1,256]{1,0:T(1,128)} %get-tuple-element.294) | copy-start | bytes 3076
  47.8 20.6 %copy-start.21 = (f32[1,256]{1,0:T(1,128)S(1)}, f32[1,256]{1,0:T(1,128)}, u32[]{:S(2)}) copy-start(f32[1,256]{1,0:T(1,128)} %get-tuple-element.295) | copy-start | bytes 3076
  47.8 20.6 %copy-start.22 = (f32[1,256]{1,0:T(1,128)S(1)}, f32[1,256]{1,0:T(1,128)}, u32[]{:S(2)}) copy-start(f32[1,256]{1,0:T(1,128)} %get-tuple-element.296) | copy-start | bytes 3076
  66.8 3.3 copy-start.1
  73.9 17.4 %copy-start.15 = (f32[4]{0:T(128)S(1)}, f32[4]{0:T(128)}, u32[]{:S(2)}) copy-start(f32[4]{0:T(128)} %copy-done.14) | copy-start | bytes 52
  73.9 17.4 %copy-start.19 = (f32[3]{0:T(128)S(1)}, f32[3]{0:T(128)}, u32[]{:S(2)}) copy-start(f32[3]{0:T(128)} %copy-done.18) | copy-start | bytes 40
  73.9 17.6 %copy-start.13 = (s32[512]{0:T(512)S(1)}, s32[512]{0:T(512)}, u32[]{:S(2)}) copy-start(s32[512]{0:T(512)} %param.30) | copy-start | bytes 6148
  97.3 2.2 copy-start.27
  103.3 2.2 copy-start.23
  103.3 158.2 %all-gather.10.cloned.1.call-start = ((), (), s32[]{:S(2)}) async-start(), calls=%async_computation.2 | async-start | bytes 7208960 | tf_op jit(solution)/shard_map/all_gather | solution.py:224
  104.1 263.8 %all-gather.12.cloned.1.call-start = ((), (), s32[]{:S(2)}) async-start(), calls=%async_computation.3 | async-start | bytes 7208960 | tf_op jit(solution)/shard_map/all_gather | solution.py:225
  104.6 369.7 %all-gather.14.cloned.1.call-start = ((), (), s32[]{:S(2)}) async-start(), calls=%async_computation.4 | async-start | bytes 7208960 | tf_op jit(solution)/shard_map/all_gather | solution.py:226
  105.2 412.0 %reduce-scatter.2.cloned.1.call-start = ((), (), s32[]{:S(2)}) async-start(), calls=%async_computation.5 | async-start | bytes 2621440 | tf_op jit(solution)/shard_map/reduce_scatter | solution.py:232
Sparse Core Ops, SparseCore 0:
  41.8 26.4 all-gather.15
  103.4 49.6 all-reduce.5
  154.7 106.7 all-gather.9
  262.9 104.9 all-gather.11
  369.3 104.9 all-gather.13
  487.8 29.4 reduce-scatter.1
where the time goes:
time: 527 us; the launch traced here: 526 us
  waiting for transfers between devices  389 us (74%)
  matrix products  32.9 us (6%)
  other arithmetic  26.9 us (5%)
  blocking collectives  18.9 us (4%)
  local copies, waits for them, and re-layouts  17.5 us (3%)
  between operations  15.4 us (3%)
  starting transfers between devices  14.8 us (3%)
  loops' own time  10.5 us (2%)
    all_gather x1, waiting for transfers between devices, on_device(): lax.all_gather(down_rows, 'sp', axis=0, tiled=True)  106 us
    all_gather x1, waiting for transfers between devices, on_device(): lax.all_gather(gate_weight, 'sp', axis=0, tiled=True)  105 us
    all_gather x1, waiting for transfers between devices, on_device(): lax.all_gather(up_weight, 'sp', axis=0, tiled=True)  98.8 us
    psum x1, waiting for transfers between devices, on_device(): mix = lax.psum(partial_value.astype(jnp.bfloat16), 'tp').astype(jnp.float32)  47.6 us
    reduce_scatter x1, waiting for transfers between devices, on_device(): lax.psum_scatter(down.astype(jnp.bfloat16), 'tp', scatter_dimension=1, ti...  29.6 us
    ppermute x4, starting transfers between devices, from_behind(): return lax.ppermute(value, axis, pairs)  14.4 us
    dot_general x1, matrix products, down_product(): lax.dot_general(hidden, rows, (((1,), (1,)), ((), ())), preferred_element...  13.3 us
  transfers between devices with their start and end apart: 10, of which 5 were waited for; matrix products, arithmetic and copies ran while one was open for 8% of the time, Pallas kernels for 0%

commit v1 on v0

--- a/solution.py
+++ b/solution.py
@@ -1,7 +1,14 @@
+import functools
+
 import jax
 import jax.numpy as jnp
 from jax import lax
+from jax.experimental import pallas as pl
+from jax.experimental.pallas import tpu as pltpu
 from jax.sharding import PartitionSpec as P
+
+
+MESH = pl.DeviceIdType.MESH
 
 HEADS = 64
 GROUPS = 8
@@ -17,27 +24,32 @@
     return lax.ppermute(value, axis, pairs)
 
 
-def prefix(value, axis, combine, identity):
+def entering_state(decay, state, first_doc, last_doc, axis):
     peers, index = (lax.axis_size(axis), lax.axis_index(axis))
-    everything = jax.tree.map(
-        lambda part, kind: lax.all_gather(part.astype(kind), axis),
-        value,
-        (jnp.bfloat16, jnp.bfloat16, jnp.bfloat16, jnp.bfloat16),
-    )
-    start = jax.tree.map(
-        lambda part, zero: jnp.broadcast_to(jnp.asarray(zero, part.dtype), part.shape),
-        value,
-        identity,
-    )
-
-    def step(k, before):
-        reached = k < index
-        new = combine(
-            before, jax.tree.map(lambda part, own: part[k].astype(own.dtype), everything, value)
-        )
-        return jax.tree.map(lambda a, b: jnp.where(reached, a, b), new, before)
-
-    return lax.fori_loop(0, peers, step, start)
+    heads = decay.size
+    lanes = state.shape[-1]
+    marks = jnp.concatenate([decay.reshape(-1), first_doc, last_doc])
+    marks = jnp.pad(marks, (0, lanes - heads - 2))
+    rows = jnp.broadcast_to(marks[None], (16, lanes))
+    packed = jnp.concatenate([state.reshape(-1, lanes), rows]).astype(jnp.bfloat16)
+    held = jnp.zeros(state.shape, jnp.float32)
+    factor = jnp.ones((heads,), jnp.float32)
+    before = jnp.full((1,), -1.0, jnp.float32)
+    later_first = None
+    for k in range(1, peers):
+        there = k <= index
+        got = from_behind(packed, axis, k)
+        marks = got[-1].astype(jnp.float32)
+        if k == 1:
+            before = jnp.where(there, marks[heads + 1 : heads + 2], before)
+        else:
+            factor = factor * (later_first == marks[heads + 1])
+        weight = jnp.where(there, factor, 0.0).reshape(decay.shape)
+        part = got[:-16].astype(jnp.float32).reshape(state.shape)
+        held = held + weight[..., None, None] * part
+        factor = factor * marks[:heads]
+        later_first = marks[heads]
+    return held, before
 
 
 def short_filter(rows, row_docs, taps):
@@ -117,25 +129,234 @@
     return taken * jnp.transpose(reach, (2, 3, 0, 1))[..., None]
 
 
-def join_states(earlier, later):
-    early_decay, early_state, early_first, early_last = earlier
-    late_decay, late_state, late_first, late_last = later
-    link = ((late_first == early_last) | (early_last < 0.0) | (late_first < 0.0)).astype(
-        jnp.float32
-    )
-    carried = late_decay * link
-    return (
-        early_decay * carried,
-        late_state + carried[..., None, None] * early_state,
-        jnp.where(early_first < 0.0, late_first, early_first),
-        jnp.where(late_last < 0.0, early_last, late_last),
-    )
-
-
 def down_product(hidden, rows):
     return lax.dot_general(
         hidden, rows, (((1,), (1,)), ((), ())), preferred_element_type=jnp.float32
     )
+
+
+def greet(peers, me):
+    barrier = pltpu.get_barrier_semaphore()
+    for off in range(1, peers):
+        pl.semaphore_signal(
+            barrier, inc=1, device_id={"tp": lax.rem(me + off, peers)}, device_id_type=MESH
+        )
+    pl.semaphore_wait(barrier, peers - 1)
+
+
+def tp_copy(src, dst, send, recv, peer):
+    return pltpu.make_async_remote_copy(
+        src_ref=src,
+        dst_ref=dst,
+        send_sem=send,
+        recv_sem=recv,
+        device_id={"tp": peer},
+        device_id_type=MESH,
+    )
+
+
+def columns_of(index, share):
+    return pl.ds(pl.multiple_of(index * share, share), share)
+
+
+def mix_kernel(
+    peers, mixer_ref, out_ref, res_ref, gain_ref, own_ref, normal_ref,
+    going, coming, own_part, shared, sums, send_a, recv_a, send_b, recv_b,
+):
+    me = lax.axis_index("tp")
+    share = own_part.shape[1]
+    greet(peers, me)
+    copies = []
+    for off in range(peers - 1, 0, -1):
+        peer = lax.rem(me + off, peers)
+        going[off - 1] = jnp.dot(
+            mixer_ref[...], out_ref[:, columns_of(peer, share)], preferred_element_type=jnp.float32
+        ).astype(jnp.bfloat16)
+        copy = tp_copy(
+            going.at[off - 1], coming.at[off - 1], send_a.at[off - 1], recv_a.at[off - 1], peer
+        )
+        copy.start()
+        copies.append(copy)
+    mine = columns_of(me, share)
+    total = (
+        jnp.dot(mixer_ref[...], out_ref[:, mine], preferred_element_type=jnp.float32)
+        .astype(jnp.bfloat16)
+        .astype(jnp.float32)
+    )
+    for copy in copies:
+        copy.wait_recv()
+    for off in range(1, peers):
+        total = total + coming[off - 1].astype(jnp.float32)
+    after = (res_ref[:, mine].astype(jnp.float32) + total).astype(jnp.bfloat16)
+    own_part[...] = after
+    own_ref[...] = after
+    later = []
+    for off in range(peers - 1, 0, -1):
+        copy = tp_copy(
+            own_part, shared.at[off - 1], send_b.at[off - 1], recv_b.at[off - 1],
+            lax.rem(me + off, peers),
+        )
+        copy.start()
+        later.append(copy)
+    wide = after.astype(jnp.float32)
+    squares = jnp.sum(wide * wide, axis=1, keepdims=True)
+    for copy in later:
+        copy.wait_recv()
+    for off in range(1, peers):
+        wide = shared[off - 1].astype(jnp.float32)
+        squares = squares + jnp.sum(wide * wide, axis=1, keepdims=True)
+    scale = lax.rsqrt(squares / (share * peers) + norm_eps)
+    normal_ref[:, mine] = (
+        own_part[...].astype(jnp.float32) * scale * gain_ref[:, mine].astype(jnp.float32)
+    ).astype(jnp.bfloat16)
+    for off in range(1, peers):
+        theirs = columns_of(lax.rem(me - off + peers, peers), share)
+        normal_ref[:, theirs] = (
+            shared[off - 1].astype(jnp.float32) * scale * gain_ref[:, theirs].astype(jnp.float32)
+        ).astype(jnp.bfloat16)
+    for copy in copies + later:
+        copy.wait_send()
+
+
+def mix_and_norm(mixer_in, mixer_out, residual, channel_gain):
+    peers = lax.axis_size("tp")
+    rows, width = residual.shape
+    share = width // peers
+    flops = 2 * rows * width * mixer_in.shape[1]
+    part = (peers - 1, rows, share)
+    return pl.pallas_call(
+    functools.partial(mix_kernel, peers),
+    out_shape=(
+        jax.ShapeDtypeStruct((rows, share), jnp.bfloat16),
+        jax.ShapeDtypeStruct((rows, width), jnp.bfloat16),
+    ),
+    in_specs=[pl.BlockSpec(memory_space=pltpu.VMEM)] * 4,
+    out_specs=[pl.BlockSpec(memory_space=pltpu.VMEM)] * 2,
+    scratch_shapes=[
+        pltpu.VMEM(part, jnp.bfloat16),
+        pltpu.VMEM(part, jnp.bfloat16),
+        pltpu.VMEM((rows, share), jnp.bfloat16),
+        pltpu.VMEM(part, jnp.bfloat16),
+        pltpu.VMEM((rows, 128), jnp.float32),
+    ]
+    + [pltpu.SemaphoreType.DMA((peers - 1,))] * 4,
+    compiler_params=pltpu.CompilerParams(
+        collective_id=0, has_side_effects=True, vmem_limit_bytes=40 * 1024 * 1024
+    ),
+    cost_estimate=pl.CostEstimate(flops=20 * flops, bytes_accessed=0, transcendentals=0),
+    name="mix_and_norm",
+    )(mixer_in, mixer_out, residual, channel_gain.reshape(1, width))
+
+
+def down_kernel(peers, part_ref, result_ref, coming, send_a, recv_a):
+    me = lax.axis_index("tp")
+    greet(peers, me)
+    copies = []
+    for off in range(peers - 1, 0, -1):
+        peer = lax.rem(me + off, peers)
+        copy = tp_copy(
+            part_ref.at[peer], coming.at[off - 1], send_a.at[off - 1], recv_a.at[off - 1], peer
+        )
+        copy.start()
+        copies.append(copy)
+    total = part_ref[me].astype(jnp.float32)
+    for copy in copies:
+        copy.wait_recv()
+    for off in range(1, peers):
+        total = total + coming[off - 1].astype(jnp.float32)
+    result_ref[...] = total
+    for copy in copies:
+        copy.wait_send()
+
+
+def add_down(parts, place):
+    peers, rows, share = parts.shape
+    return pl.pallas_call(
+        functools.partial(down_kernel, peers),
+        out_shape=jax.ShapeDtypeStruct((rows, share), jnp.float32),
+        in_specs=[pl.BlockSpec(memory_space=pltpu.VMEM)],
+        out_specs=pl.BlockSpec(memory_space=pltpu.VMEM),
+        scratch_shapes=[pltpu.VMEM((peers - 1, rows, share), jnp.bfloat16)]
+        + [pltpu.SemaphoreType.DMA((peers - 1,))] * 2,
+        compiler_params=pltpu.CompilerParams(collective_id=place, has_side_effects=True),
+    )(parts)
+
+
+def gather_weights(weights):
+    first = lax.axis_index("grp")
+    columns = weights[0].shape[1]
+    half = -(-columns // 256) * 128
+    rest = columns - half
+    near, local = [], []
+    rows = weights[2].shape[0] // 2
+    pieces = (weights[0], weights[1], weights[2][:rows], weights[2][rows:])
+    for weight in pieces:
+        piece = lax.dynamic_slice_in_dim(weight, first * rest, half, 1)
+        near.append(lax.all_gather(piece, "sp", axis=0))
+        local.append(lax.dynamic_slice_in_dim(weight, (1 - first) * half, rest, 1))
+    return near, local
+
+
+def swap(gathered, columns):
+    steps, rows, half = gathered.shape
+    index, first = (lax.axis_index("sp"), lax.axis_index("grp"))
+    lead = first * (2 * half - columns)
+    turn = [
+        lax.dynamic_slice(
+            gathered, (lax.rem(index + k, steps), 0, lead), (1, rows, columns - half)
+        )
+        for k in range(1, steps)
+    ]
+    return lax.ppermute(jnp.concatenate(turn).reshape(-1, columns - half), "grp", [(0, 1), (1, 0)])
+
+
+def turned(array, by):
+    return lax.dynamic_slice_in_dim(
+        jnp.concatenate([array, array], axis=1), by, array.shape[1], 1
+    )
+
+
+def channel_mixer(normal, own_after, near, local, far):
+    tokens, _ = normal.shape
+    rows = local[0].shape[0]
+    half = near[0].shape[2]
+    here = lax.axis_index("sp") * rows
+    mine = turned(normal, here)
+
+    def product(k):
+        return jnp.dot(
+            mine[:, :rows], local[k], preferred_element_type=jnp.float32
+        ) + jnp.dot(mine[:, rows:], far[k], preferred_element_type=jnp.float32)
+
+    whole = [weight.reshape(-1, weight.shape[2]) for weight in near]
+    gate = jnp.dot(normal, whole[0], preferred_element_type=jnp.float32)
+    up = jnp.dot(normal, whole[1], preferred_element_type=jnp.float32)
+    hidden = (jax.nn.silu(gate) * up).astype(jnp.bfloat16)
+    columns = half + far[0].shape[1]
+    late, hidden = lax.optimization_barrier((near[2], hidden))
+    far_low = swap(late, columns)
+    last, far_low = lax.optimization_barrier((near[3], far_low))
+    far_high = swap(last, columns)
+    others = (jax.nn.silu(product(0)) * product(1)).astype(jnp.bfloat16)
+
+    def down_part(here_rows, gathered, swapped, kept, name):
+        steps, count, _ = gathered.shape
+        down_near = down_product(hidden, gathered.reshape(-1, half))
+        down_far = jnp.concatenate(
+            [down_product(others, kept), down_product(others, swapped)], axis=1
+        )
+        down = down_near + turned(down_far, steps * count - here_rows)
+        peers = lax.axis_size("tp")
+        share = steps * count // peers
+        parts = jnp.stack(
+            [down[:, k * share : (k + 1) * share].astype(jnp.bfloat16) for k in range(peers)]
+        )
+        return add_down(parts, name).reshape(tokens, -1, count)
+
+    low = down_part(here // 2, late, far_low, local[2], 1)
+    high = down_part(here // 2, last, far_high, local[3], 2)
+    down = jnp.concatenate([low, high], axis=2).reshape(own_after.shape)
+    return (own_after.astype(jnp.float32) + down).astype(jnp.bfloat16)
 
 
 def on_device(
@@ -158,18 +379,25 @@
     up_weight,
     down_rows,
 ):
+    near, local = gather_weights((gate_weight, up_weight, down_rows))
     tokens = values.shape[0]
     edge = taps_values.shape[0] - 1
     segment = documents.astype(jnp.float32)
-    before = from_behind(
-        (
-            values[tokens - edge :],
-            writes[tokens - edge :],
-            reads[tokens - edge :],
-            segment[tokens - edge :].astype(jnp.bfloat16),
+    wide, narrow = values.shape[1], writes.shape[1]
+    tail_docs = jnp.broadcast_to(segment[tokens - edge :, None], (edge, 128)).astype(jnp.bfloat16)
+    behind = from_behind(
+        jnp.concatenate(
+            [values[tokens - edge :], writes[tokens - edge :], reads[tokens - edge :], tail_docs],
+            axis=1,
         ),
         "sp",
         1,
+    )
+    before = (
+        behind[:, :wide],
+        behind[:, wide : wide + narrow],
+        behind[:, wide + narrow : wide + 2 * narrow],
+        behind[:, wide + 2 * narrow],
     )
     row_docs = jnp.concatenate([before[3].astype(jnp.float32), segment])
     short_values = short_filter(jnp.concatenate([before[0], values]), row_docs, taps_values)
@@ -190,15 +418,10 @@
     whole_decay = jnp.exp(jnp.sum(last_total, axis=2)) * (segment[0] == segment[-1]).astype(
         jnp.float32
     )
-    identity = (
-        jnp.ones_like(whole_decay),
-        zero_state,
-        jnp.full((1,), -1.0, jnp.float32),
-        jnp.full((1,), -1.0, jnp.float32),
-    )
-    scanned = prefix((whole_decay, final, segment[:1], segment[-1:]), "sp", join_states, identity)
-    held = scanned[1]
-    prior_docs = jnp.concatenate([scanned[3], block_docs[:-1, -1]])
+    held, before_doc = entering_state(whole_decay, final, segment[:1], segment[-1:], "sp")
+    early, held = lax.optimization_barrier((near[0], held))
+    far_gate = swap(early, gate_weight.shape[1])
+    prior_docs = jnp.concatenate([before_doc, block_docs[:-1, -1]])
     passing_in = block_passing(last_total, block_docs, prior_docs)
     gains = jnp.cumprod(passing_in, axis=2)
     gains = jnp.concatenate([jnp.ones_like(gains[..., :1]), gains[..., :-1]], axis=2)
@@ -210,29 +433,10 @@
     mixer_in = (grouped.reshape(tokens, -1) * mixer_gain.astype(jnp.float32)[None, :]).astype(
         jnp.bfloat16
     )
-    partial_value = jnp.dot(mixer_in, mixer_out, preferred_element_type=jnp.float32)
-    share = residual.shape[1] // lax.axis_size("tp")
-    mix = lax.psum(partial_value.astype(jnp.bfloat16), "tp").astype(jnp.float32)
-    after = (residual.astype(jnp.float32) + mix).astype(jnp.bfloat16)
-    own_after = lax.dynamic_slice_in_dim(after, lax.axis_index("tp") * share, share, 1)
-    after_wide = after.astype(jnp.float32)
-    normal = after_wide * lax.rsqrt(
-        jnp.mean(after_wide * after_wide, axis=1, keepdims=True) + norm_eps
-    )
-    normal = (normal * channel_gain.astype(jnp.float32)[None, :]).astype(jnp.bfloat16)
-    late_weights = (
-        lax.all_gather(gate_weight, "sp", axis=0, tiled=True),
-        lax.all_gather(up_weight, "sp", axis=0, tiled=True),
-        lax.all_gather(down_rows, "sp", axis=0, tiled=True),
-    )
-    gate = jnp.dot(normal, late_weights[0], preferred_element_type=jnp.float32)
-    up = jnp.dot(normal, late_weights[1], preferred_element_type=jnp.float32)
-    hidden = (jax.nn.silu(gate) * up).astype(jnp.bfloat16)
-    down = down_product(hidden, late_weights[2])
-    down_share = lax.psum_scatter(
-        down.astype(jnp.bfloat16), "tp", scatter_dimension=1, tiled=True
-    ).astype(jnp.float32)
-    return (own_after.astype(jnp.float32) + down_share).astype(jnp.bfloat16)
+    own_after, normal = mix_and_norm(mixer_in, mixer_out, residual, channel_gain)
+    middle, far_gate, normal = lax.optimization_barrier((near[1], far_gate, normal))
+    far_up = swap(middle, gate_weight.shape[1])
+    return channel_mixer(normal, own_after, near, local, (far_gate, far_up))
 
 
 def solution(mesh):

time: 527 us -> 312 us (0.59)
  the two profiles are of different devices: /device:TPU:0 before, /device:TPU:16 now
where the time goes in v1:
time: 312 us; the launch traced here: 310 us
  Pallas kernels  83.1 us (27%)
  waiting for transfers between devices  68.7 us (22%)
  other arithmetic  50.6 us (16%)
  local copies, waits for them, and re-layouts  42.8 us (14%)
  matrix products  34.2 us (11%)
  between operations  18.6 us (6%)
  starting transfers between devices  12.1 us (4%)
    pallas_call x1, Pallas kernels, mix_and_norm(): pl.pallas_call(functools.partial(mix_kernel, peers), out_shape=(jax.Shape...  50.2 us
    pallas_call x2, Pallas kernels, add_down(): pl.pallas_call(functools.partial(down_kernel, peers), out_shape=jax.Shape...  32.9 us
    all_gather x4, waiting for transfers between devices, gather_weights(): near.append(lax.all_gather(piece, 'sp', axis=0))  23.8 us
    ppermute x4, waiting for transfers between devices, from_behind(): return lax.ppermute(value, axis, pairs)  23.7 us
    ppermute x4, waiting for transfers between devices, swap(): lax.ppermute(jnp.concatenate(turn).reshape(-1, columns - half), 'grp', [(...  21.1 us
    dot_general x6, matrix products, down_product(): lax.dot_general(hidden, rows, (((1,), (1,)), ((), ())), preferred_element...  10.9 us
    convert_element_type x3, other arithmetic, short_filter(): return jax.nn.silu(total).astype(jnp.bfloat16)  8.35 us
    ppermute x4, starting transfers between devices, from_behind(): return lax.ppermute(value, axis, pairs)  8.22 us
  transfers between devices with their start and end apart: 12, of which 4 were waited for; matrix products, arithmetic and copies ran while one was open for 36% of the time, Pallas kernels for 21%

profile of v1, /device:TPU:16, one launch (start us, length us, event | category | flops | bytes accessed | tf_op | source)
XLA Modules:
  0.0 310.1 jit_solution(4437716563146856212)
XLA Ops:
  6.5 1.4 copy-done
  10.1 1.5 fusion.88
  14.9 3.5 %collective-permute-start = (bf16[3,1664]{1,0:T(4,128)(2,1)S(1)}, bf16[3,1664]{1,0:T(4,128)(2,1)S(1)}, u32[]{:S(2)}, u32[]{:S(2)}) collective-permute-start(bf16[3,1664]{1,0:T(4,128)(2,1)S(1)} %pad_maximum_fusion.10), channel_id=1, source_target_pairs={{0,4},{4,8},{8,12},{1,5},{5,9},{9,13},{2,6},{6,10},{10,14},{3,7},{... | collective-permute-start | bytes 29960 | tf_op jit(solution)/shard_map/ppermute | solution.py:24
  20.3 2.3 reduce_window_sum.11
  27.6 1.9 fusion.85
  31.2 5.2 %multiply_convert_fusion.4 = bf16[512,1024]{1,0:T(8,128)(2,1)S(1)} fusion(bf16[512,1024]{1,0:T(8,128)(2,1)} %param.21, bf16[3,1024]{1,0:T(4,128)(2,1)S(1)} %slice.304, f32[512]{0:T(512)S(1)} %get-tuple-element.157, f32[1024]{0:T(1024)S(1)} %bitcast.138, f32[512]{0:T(512)S(1)} %get-tuple-element.147, f32[1024]{0:T(1024)S(1)} %bitcast.139, ...), kind=kLoop, calls=%fused_computation.44 | loop fusion | flops 15204352 | bytes 2127872 | tf_op jit(solution)/shard_map/convert_element_type | solution.py:68
  36.3 1.3 copy.98
  37.7 1.3 reshape.253
  40.9 1.3 multiply_convert_fusion.3
  42.1 1.8 fusion.42
  44.0 10.8 %while.13 = (s32[]{:T(128)}, f32[2,8,64,128]{3,2,1,0:T(8,128)S(1)}, f32[4,2,8,64,128]{4,3,2,1,0:T(8,128)}, f32[4,2,8]{2,0,1:T(4,128)}, f32[4,2,8,64,128]{4,3,2,1,0:T(8,128)}, /*index=5*/s32[]{:T(128)}, s32[]{:T(128)}) while((s32[]{:T(128)}, f32[2,8,64,128]{3,2,1,0:T(8,128)S(1)}, f32[4,2,8,64,128]{4,3,2,1,0:T(8,128)}, ...), condition=%wide.region_2.3_spmd.clone, body=%wide.region_1.2_spmd.clone.sunk | while | flops 524291 | bytes 2622240 | solution.py:118
  55.7 1.3 collective-permute-start.2
  57.0 1.4 collective-permute-start.3
  58.3 2.1 collective-permute-start.1
  60.5 2.0 multiply_convert_fusion.8
  63.0 3.0 fusion
  66.0 1.3 slice.328
  67.3 6.4 %collective-permute-done.2 = bf16[1040,128]{1,0:T(8,128)(2,1)} collective-permute-done((bf16[1040,128]{1,0:T(8,128)(2,1)}, bf16[1040,128]{1,0:T(8,128)(2,1)}, u32[]{:S(2)}, u32[]{:S(2)}) %collective-permute-start.2) | collective-permute-done | bytes 266272 | tf_op jit(solution)/shard_map/ppermute | solution.py:24
  76.4 17.3 %collective-permute-done.1 = bf16[1040,128]{1,0:T(8,128)(2,1)} collective-permute-done((bf16[1040,128]{1,0:T(8,128)(2,1)}, bf16[1040,128]{1,0:T(8,128)(2,1)}, u32[]{:S(2)}, u32[]{:S(2)}) %collective-permute-start.1) | collective-permute-done | bytes 266272 | tf_op jit(solution)/shard_map/ppermute | solution.py:24
  102.6 3.8 %fusion.16 = f32[4,128,2,8,64]{1,4,3,2,0:T(8,128)S(1)} fusion(f32[4,2,8,64,128]{4,3,2,1,0:T(8,128)} %fusion, f32[4,2,8,64,128]{4,3,2,1,0:T(8,128)} %get-tuple-element.44, f32[2,8,64,128]{3,2,1,0:T(8,128)} %fusion.51, f32[4,2,8]{2,1,0:T(2,128)S(1)} %copy.109, bf16[4,128,2,128,1]{3,2,1,0,4:T(2,128)(2,1)} %bitcast.123, f32[2,8,4,128]{3,1,2,0:T(8,128)} %copy-done.18, ...), kind=kOutput, calls=%fused_computation.33 | convolution fusion | flops 807411712 | bytes 7112960 | tf_op jit(solution)/shard_map/kign,kgepn->kigep/dot_general | solution.py:128
  106.4 3.0 copy.128
  109.4 3.5 %reshape.306 = f32[512,1024]{1,0:T(8,128)S(1)} reshape(f32[4,128,2,8,64]{4,3,2,1,0:T(8,128)} %copy.128) | data formatting | bytes 4194304 | tf_op jit(solution)/shard_map/reshape | solution.py:430
  112.9 3.1 %fusion.87 = f32[512,1024]{1,0:T(8,128)} fusion(f32[512,1024]{1,0:T(8,128)S(1)} %reshape.306, bf16[512,1024]{1,0:T(8,128)(2,1)} %param.22), kind=kLoop, calls=%fused_computation.201 | loop fusion | flops 3670016 | bytes 5242880 | tf_op jit(solution)/shard_map/mul | solution.py:432
  116.1 4.0 %mul.606 = f32[512,2,512]{2,1,0:T(2,128)} reshape(f32[512,1024]{1,0:T(8,128)} %fusion.87) | data formatting | bytes 4194304 | tf_op jit(solution)/shard_map/mul | solution.py:432
  120.1 3.0 reduce_sum.19
  125.5 1.4 copy-done.13
  127.1 1.5 pad_maximum_fusion
  128.7 1.6 collective-permute-start.4
  131.1 1.4 copy-done.3
  133.2 50.2 %mix_and_norm.1 = (bf16[512,512]{1,0:T(8,128)(2,1)S(1)}, bf16[512,2048]{1,0:T(8,128)(2,1)S(1)}) custom-call(bf16[512,1024]{1,0:T(8,128)(2,1)S(1)} %multiply_convert_fusion.2.mixer_ref, bf16[1024,2048]{1,0:T(8,128)(2,1)S(1)} %copy-done.3, bf16[512,2048]{1,0:T(8,128)(2,1)S(1)} %copy-done.4, bf16[1,2048]{1,0:T(2,128)(2,1)S(1)} %reshape.263.gain_ref), custom_call_target="tpu_custom_call" | custom-call | flops 42949672960 | tf_op jit(solution)/shard_map/mix_and_norm/pallas_call | solution.py:227
  184.2 1.7 constant_dynamic-slice_fusion.10
  185.8 1.6 pad_maximum_fusion.1
  188.4 1.8 fusion.93
  190.2 2.8 multiply_convert_fusion.5
  198.2 1.8 fusion.47
  200.0 4.4 %fusion.32 = f32[512,640]{1,0:T(8,128)} fusion(f32[512,640]{1,0:T(8,128)S(1)} %fusion.49, bf16[1536,640]{1,0:T(8,128)(2,1)} %collective-permute-done.4, bf16[512,2048]{1,0:T(8,128)(2,1)S(1)} %fusion.15), kind=kOutput, calls=%fused_computation.55 | convolution fusion | flops 1006960640 | bytes 6160384 | tf_op jit(solution)/shard_map/dot_general | solution.py:329
  204.4 23.8 %all-gather.15.cloned.1.call-done = bf16[1024,768]{1,0:T(8,128)(2,1)} async-done(((bf16[256,768]{1,0:T(8,128)(2,1)}), bf16[1024,768]{1,0:T(8,128)(2,1)}) %all-gather.15.cloned.1.call-update) | async-done | bytes 1572880 | tf_op jit(solution)/shard_map/all_gather | solution.py:295
  228.2 21.1 %collective-permute-done.6 = bf16[768,640]{1,0:T(8,128)(2,1)} collective-permute-done((bf16[768,640]{1,0:T(8,128)(2,1)}, bf16[768,640]{1,0:T(8,128)(2,1)}, u32[]{:S(2)}, u32[]{:S(2)}) %collective-permute-start.6) | collective-permute-done | bytes 983072 | tf_op jit(solution)/shard_map/ppermute | solution.py:310
  252.3 3.0 multiply_convert_fusion.6
  255.4 1.5 fusion.57
  256.9 2.0 fusion.94
  258.9 1.9 fusion.14
  262.1 16.4 %shard_map.172 = f32[512,256]{1,0:T(8,128)} custom-call(bf16[4,512,256]{2,1,0:T(8,128)(2,1)} %pad_maximum_fusion.3.part_ref), custom_call_target="tpu_custom_call" | custom-call | tf_op jit(solution)/shard_map/pallas_call | solution.py:274
  278.5 1.5 fusion.55
  280.0 2.0 fusion.95
  282.1 1.9 fusion.9
  285.2 16.4 %shard_map.173 = f32[512,256]{1,0:T(8,128)} custom-call(bf16[4,512,256]{2,1,0:T(8,128)(2,1)} %pad_maximum_fusion.4.part_ref), custom_call_target="tpu_custom_call" | custom-call | tf_op jit(solution)/shard_map/pallas_call | solution.py:274
  301.6 2.0 fusion.41
  (212 shorter events, 51.0 us)
Async XLA Ops:
  6.5 96.1 %all-gather.9.cloned.1.call-start = ((), (), s32[]{:S(2)}) async-start(), calls=%async_computation | async-start | bytes 3932160 | tf_op jit(solution)/shard_map/all_gather | solution.py:295
  8.9 175.3 %all-gather.13.cloned.1.call-start = ((), (), s32[]{:S(2)}) async-start(), calls=%async_computation.2 | async-start | bytes 3932160 | tf_op jit(solution)/shard_map/all_gather | solution.py:295
  10.0 4.2 %copy-start.20 = (bf16[512,256]{1,0:T(8,128)(2,1)S(1)}, bf16[512,256]{1,0:T(8,128)(2,1)}, u32[]{:S(2)}) copy-start(bf16[512,256]{1,0:T(8,128)(2,1)} %param.23) | copy-start | bytes 786436
  10.0 9.6 %copy-start.25 = (bf16[4,1024]{1,0:T(4,128)(2,1)S(1)}, bf16[4,1024]{1,0:T(4,128)(2,1)}, u32[]{:S(2)}) copy-start(bf16[4,1024]{1,0:T(4,128)(2,1)} %param.29) | copy-start | bytes 24580
  10.0 9.7 %copy-start.22 = (bf16[16,512]{1,0:T(8,128)(2,1)S(1)}, bf16[16,512]{1,0:T(8,128)(2,1)}, u32[]{:S(2)}) copy-start(bf16[16,512]{1,0:T(8,128)(2,1)} %param.25) | copy-start | bytes 49156
  10.0 9.7 %copy-start.23 = (f32[16,512]{1,0:T(8,128)S(1)}, f32[16,512]{1,0:T(8,128)}, u32[]{:S(2)}) copy-start(f32[16,512]{1,0:T(8,128)} %param.27) | copy-start | bytes 98308
  10.0 9.7 %copy-start.51 = (f32[16]{0:T(128)S(1)}, f32[16]{0:T(128)}, u32[]{:S(2)}) copy-start(f32[16]{0:T(128)} %param.26) | copy-start | bytes 196
  10.0 12.8 %copy-start.40 = (bf16[4,256]{1,0:T(4,128)(2,1)S(1)}, bf16[4,256]{1,0:T(4,128)(2,1)}, u32[]{:S(2)}) copy-start(bf16[4,256]{1,0:T(4,128)(2,1)} %param.30) | copy-start | bytes 6148
  10.0 183.0 %all-gather.11.cloned.1.call-start = ((), (), s32[]{:S(2)}) async-start(), calls=%async_computation.1 | async-start | bytes 1966080 | tf_op jit(solution)/shard_map/all_gather | solution.py:295
  11.6 18.0 %copy-start.8 = (bf16[256,1408]{1,0:T(8,128)(2,1)}, bf16[256,1408]{1,0:T(8,128)(2,1)S(1)}, u32[]{:S(2)}) copy-start(bf16[256,1408]{1,0:T(8,128)(2,1)S(1)} %get-tuple-element.129) | copy-start | bytes 2162692
  11.6 14.7 %copy-start.41 = (bf16[4,256]{1,0:T(4,128)(2,1)S(1)}, bf16[4,256]{1,0:T(4,128)(2,1)}, u32[]{:S(2)}) copy-start(bf16[4,256]{1,0:T(4,128)(2,1)} %param.31) | copy-start | bytes 6148
  11.6 18.6 %copy-start.49 = (bf16[1024]{0:T(1024)(128)(2,1)S(1)}, bf16[1024]{0:T(1024)(128)(2,1)}, u32[]{:S(2)}) copy-start(bf16[1024]{0:T(1024)(128)(2,1)} %param.32) | copy-start | bytes 6148
  11.6 19.2 %copy-start.48 = (bf16[2048]{0:T(1024)(128)(2,1)S(1)}, bf16[2048]{0:T(1024)(128)(2,1)}, u32[]{:S(2)}) copy-start(bf16[2048]{0:T(1024)(128)(2,1)} %param.34) | copy-start | bytes 12292
  13.3 215.0 %all-gather.15.cloned.1.call-start = ((), (), s32[]{:S(2)}) async-start(), calls=%async_computation.3 | async-start | bytes 1966080 | tf_op jit(solution)/shard_map/all_gather | solution.py:295
  14.9 15.9 %collective-permute-start = (bf16[3,1664]{1,0:T(4,128)(2,1)S(1)}, bf16[3,1664]{1,0:T(4,128)(2,1)S(1)}, u32[]{:S(2)}, u32[]{:S(2)}) collective-permute-start(bf16[3,1664]{1,0:T(4,128)(2,1)S(1)} %pad_maximum_fusion.10), channel_id=1, source_target_pairs={{0,4},{4,8},{8,12},{1,5},{5,9},{9,13},{2,6},{6,10},{10,14},{3,7},{... | collective-permute-start | bytes 29960 | tf_op jit(solution)/shard_map/ppermute | solution.py:24
  19.4 18.2 %copy-start.38 = (f32[4]{0:T(128)}, f32[4]{0:T(128)S(1)}, u32[]{:S(2)}) copy-start(f32[4]{0:T(128)S(1)} %slice_reduce_fusion.3) | copy-start | bytes 52
  19.6 18.0 %copy-start.42 = (f32[3]{0:T(128)}, f32[3]{0:T(128)S(1)}, u32[]{:S(2)}) copy-start(f32[3]{0:T(128)S(1)} %slice_reduce_fusion.2) | copy-start | bytes 40
  22.6 8.6 %copy-start.18 = (f32[2,8,4,128]{3,1,2,0:T(8,128)}, f32[2,8,4,128]{3,1,2,0:T(8,128)S(1)}, u32[]{:S(2)}) copy-start(f32[2,8,4,128]{3,1,2,0:T(8,128)S(1)} %reduce_window_sum.11) | copy-start | bytes 98308
  31.1 6.5 %copy-start.27 = (f32[512]{0:T(512)}, f32[512]{0:T(512)S(1)}, u32[]{:S(2)}) copy-start(f32[512]{0:T(512)S(1)} %get-tuple-element.146) | copy-start | bytes 6148
  31.1 6.5 %copy-start.29 = (f32[512]{0:T(512)}, f32[512]{0:T(512)S(1)}, u32[]{:S(2)}) copy-start(f32[512]{0:T(512)S(1)} %get-tuple-element.147) | copy-start | bytes 6148
  31.1 6.5 %copy-start.31 = (f32[512]{0:T(512)}, f32[512]{0:T(512)S(1)}, u32[]{:S(2)}) copy-start(f32[512]{0:T(512)S(1)} %get-tuple-element.148) | copy-start | bytes 6148
  31.1 6.6 %copy-start.33 = (f32[512]{0:T(512)}, f32[512]{0:T(512)S(1)}, u32[]{:S(2)}) copy-start(f32[512]{0:T(512)S(1)} %get-tuple-element.157) | copy-start | bytes 6148
  43.9 11.0 %copy-start.50 = (bf16[128]{0:T(256)(128)(2,1)S(1)}, bf16[128]{0:T(256)(128)(2,1)}, u32[]{:S(2)}) copy-start(bf16[128]{0:T(256)(128)(2,1)} %fusion.85) | copy-start | bytes 772
  43.9 16.5 %copy-start.28 = (f32[512]{0:T(512)S(1)}, f32[512]{0:T(512)}, u32[]{:S(2)}) copy-start(f32[512]{0:T(512)} %copy-done.27) | copy-start | bytes 6148
  43.9 16.5 %copy-start.30 = (f32[512]{0:T(512)S(1)}, f32[512]{0:T(512)}, u32[]{:S(2)}) copy-start(f32[512]{0:T(512)} %copy-done.29) | copy-start | bytes 6148
  43.9 16.5 %copy-start.32 = (f32[512]{0:T(512)S(1)}, f32[512]{0:T(512)}, u32[]{:S(2)}) copy-start(f32[512]{0:T(512)} %copy-done.31) | copy-start | bytes 6148
  43.9 16.5 %copy-start.34 = (f32[512]{0:T(512)S(1)}, f32[512]{0:T(512)}, u32[]{:S(2)}) copy-start(f32[512]{0:T(512)} %copy-done.33) | copy-start | bytes 6148
  44.0 16.5 %copy-start.37 = (bf16[3,256]{1,0:T(4,128)(2,1)S(1)}, bf16[3,256]{1,0:T(4,128)(2,1)}, u32[]{:S(2)}) copy-start(bf16[3,256]{1,0:T(4,128)(2,1)} %get-tuple-element.140) | copy-start | bytes 4612
  44.0 16.5 %copy-start.44 = (f32[1,256]{1,0:T(1,128)S(1)}, f32[1,256]{1,0:T(1,128)}, u32[]{:S(2)}) copy-start(f32[1,256]{1,0:T(1,128)} %get-tuple-element.149) | copy-start | bytes 3076
  44.0 16.5 %copy-start.45 = (f32[1,256]{1,0:T(1,128)S(1)}, f32[1,256]{1,0:T(1,128)}, u32[]{:S(2)}) copy-start(f32[1,256]{1,0:T(1,128)} %get-tuple-element.150) | copy-start | bytes 3076
  44.0 16.5 %copy-start.46 = (f32[1,256]{1,0:T(1,128)S(1)}, f32[1,256]{1,0:T(1,128)}, u32[]{:S(2)}) copy-start(f32[1,256]{1,0:T(1,128)} %get-tuple-element.151) | copy-start | bytes 3076
  44.0 16.5 %copy-start.47 = (f32[1,256]{1,0:T(1,128)S(1)}, f32[1,256]{1,0:T(1,128)}, u32[]{:S(2)}) copy-start(f32[1,256]{1,0:T(1,128)} %get-tuple-element.152) | copy-start | bytes 3076
  54.9 8.1 %copy-start.19 = (f32[2,8,4,128]{3,1,2,0:T(8,128)S(1)}, f32[2,8,4,128]{3,1,2,0:T(8,128)}, u32[]{:S(2)}) copy-start(f32[2,8,4,128]{3,1,2,0:T(8,128)} %copy-done.18) | copy-start | bytes 98308
  54.9 8.1 %copy-start.21 = (pred[4,128,128]{2,1,0:T(8,128)(4,1)S(1)}, pred[4,128,128]{2,1,0:T(8,128)(4,1)}, u32[]{:S(2)}) copy-start(pred[4,128,128]{2,1,0:T(8,128)(4,1)} %compare_and_fusion) | copy-start | bytes 196612
  54.9 8.1 %copy-start.24 = (f32[2,8,4,128]{3,1,2,0:T(8,128)S(1)}, f32[2,8,4,128]{3,1,2,0:T(8,128)}, u32[]{:S(2)}) copy-start(f32[2,8,4,128]{3,1,2,0:T(8,128)} %get-tuple-element.138) | copy-start | bytes 98308
  55.7 18.1 %collective-permute-start.2 = (bf16[1040,128]{1,0:T(8,128)(2,1)}, bf16[1040,128]{1,0:T(8,128)(2,1)}, u32[]{:S(2)}, u32[]{:S(2)}) collective-permute-start(bf16[1040,128]{1,0:T(8,128)(2,1)} %pad_maximum_fusion.7), channel_id=1, source_target_pairs={{0,8},{4,12},{1,9},{5,13},{2,10},{6,14},{3,11},{7,15},{16,24},{20,... | collective-permute-start | bytes 798728 | tf_op jit(solution)/shard_map/ppermute | solution.py:24
  57.0 9.0 %collective-permute-start.3 = (bf16[1040,128]{1,0:T(8,128)(2,1)}, bf16[1040,128]{1,0:T(8,128)(2,1)}, u32[]{:S(2)}, u32[]{:S(2)}) collective-permute-start(bf16[1040,128]{1,0:T(8,128)(2,1)} %pad_maximum_fusion.7), channel_id=1, source_target_pairs={{0,12},{1,13},{2,14},{3,15},{16,28},{17,29},{18,30},{19,31}} | collective-permute-start | bytes 798728 | tf_op jit(solution)/shard_map/ppermute | solution.py:24
  58.3 35.3 %collective-permute-start.1 = (bf16[1040,128]{1,0:T(8,128)(2,1)}, bf16[1040,128]{1,0:T(8,128)(2,1)}, u32[]{:S(2)}, u32[]{:S(2)}) collective-permute-start(bf16[1040,128]{1,0:T(8,128)(2,1)} %pad_maximum_fusion.7), channel_id=1, source_target_pairs={{0,4},{4,8},{8,12},{1,5},{5,9},{9,13},{2,6},{6,10},{10,14},{3,7},{... | collective-permute-start | bytes 798728 | tf_op jit(solution)/shard_map/ppermute | solution.py:24
  63.0 34.8 %copy-start.39 = (f32[4]{0:T(128)S(1)}, f32[4]{0:T(128)}, u32[]{:S(2)}) copy-start(f32[4]{0:T(128)} %copy-done.38) | copy-start | bytes 52
  63.0 34.8 %copy-start.43 = (f32[3]{0:T(128)S(1)}, f32[3]{0:T(128)}, u32[]{:S(2)}) copy-start(f32[3]{0:T(128)} %copy-done.42) | copy-start | bytes 40
  128.7 55.5 %collective-permute-start.4 = (bf16[1536,640]{1,0:T(8,128)(2,1)}, bf16[1536,640]{1,0:T(8,128)(2,1)}, u32[]{:S(2)}, u32[]{:S(2)}) collective-permute-start(bf16[1536,640]{1,0:T(8,128)(2,1)} %bitcast.35), channel_id=1, source_target_pairs={{0,16},{16,0},{1,17},{17,1},{2,18},{18,2},{3,19},{19,3},{4,20},{20... | collective-permute-start | bytes 5898248 | tf_op jit(solution)/shard_map/ppermute | solution.py:310
  187.4 64.9 %collective-permute-start.5 = (bf16[1536,640]{1,0:T(8,128)(2,1)}, bf16[1536,640]{1,0:T(8,128)(2,1)}, u32[]{:S(2)}, u32[]{:S(2)}) collective-permute-start(bf16[1536,640]{1,0:T(8,128)(2,1)} %bitcast.37), channel_id=1, source_target_pairs={{0,16},{16,0},{1,17},{17,1},{2,18},{18,2},{3,19},{19,3},{4,20},{20... | collective-permute-start | bytes 5898248 | tf_op jit(solution)/shard_map/ppermute | solution.py:310
  195.4 53.9 %collective-permute-start.6 = (bf16[768,640]{1,0:T(8,128)(2,1)}, bf16[768,640]{1,0:T(8,128)(2,1)}, u32[]{:S(2)}, u32[]{:S(2)}) collective-permute-start(bf16[768,640]{1,0:T(8,128)(2,1)} %bitcast.39), channel_id=1, source_target_pairs={{0,16},{16,0},{1,17},{17,1},{2,18},{18,2},{3,19},{19,3},{4,20},{20... | collective-permute-start | bytes 2949128 | tf_op jit(solution)/shard_map/ppermute | solution.py:310
  228.2 24.1 %copy-start.6 = (bf16[512,2048]{1,0:T(8,128)(2,1)S(1)}, bf16[512,2048]{1,0:T(8,128)(2,1)}, u32[]{:S(2)}) copy-start(bf16[512,2048]{1,0:T(8,128)(2,1)} %copy-done.5) | copy-start | bytes 6291460
  228.2 24.1 %copy-start.52 = (f32[512,640]{1,0:T(8,128)S(1)}, f32[512,640]{1,0:T(8,128)}, u32[]{:S(2)}) copy-start(f32[512,640]{1,0:T(8,128)} %fusion.32) | copy-start | bytes 3932164
  251.6 28.4 %collective-permute-start.7 = (bf16[768,640]{1,0:T(8,128)(2,1)}, bf16[768,640]{1,0:T(8,128)(2,1)}, u32[]{:S(2)}, u32[]{:S(2)}) collective-permute-start(bf16[768,640]{1,0:T(8,128)(2,1)} %bitcast.46), channel_id=1, source_target_pairs={{0,16},{16,0},{1,17},{17,1},{2,18},{18,2},{3,19},{19,3},{4,20},{20... | collective-permute-start | bytes 2949128 | tf_op jit(solution)/shard_map/ppermute | solution.py:310
  284.1 17.6 %copy-start.2 = (bf16[512,512]{1,0:T(8,128)(2,1)S(1)}, bf16[512,512]{1,0:T(8,128)(2,1)}, u32[]{:S(2)}) copy-start(bf16[512,512]{1,0:T(8,128)(2,1)} %copy-done.1) | copy-start | bytes 1572868
  284.1 17.6 %copy-start.11 = (f32[512,256]{1,0:T(8,128)S(1)}, f32[512,256]{1,0:T(8,128)}, u32[]{:S(2)}) copy-start(f32[512,256]{1,0:T(8,128)} %shard_map.172) | copy-start | bytes 1572868
  (18 other events, 47.9 us)
Sparse Core Ops, SparseCore 0:
  9.0 67.3 all-gather.8
  78.0 75.3 all-gather.12
  154.9 35.8 all-gather.10
  192.3 35.8 all-gather.14
